TPU v7x, 512 devices: a 4x2x32 block of a 4x8x32 slice. The times are simulated.
512 devices in a mesh: grp: 2 (over y), sp: 32 (over z), tp: 8 (over x, core).
Axes of the slice: x: 4, y: 2, z: 32, core: 2. Of those that a mesh axis runs over, the one named last changes fastest.
The devices are a block of a 4x8x32 slice.
Arguments:
- starting_stream: bfloat16 [24576, 2048], P(('grp', 'sp'), 'tp'), parts along dimension 0, may hold values from -45 to 45
- multiplier_matrix: bfloat16 [2, 2048, 2048], P(None, 'sp', 'tp'), may hold values from -0.125 to 0.125
- memory_path_matrix: bfloat16 [2, 2048, 2048], P(None, 'sp', 'tp'), may hold values from -0.125 to 0.125
- filter_coefficients: bfloat16 [2, 4, 2048], P(None, None, 'tp'), may hold values from -3 to 3
- memory_valve_matrix: bfloat16 [2, 8, 256, 256], P(None, 'tp'), may hold values from -0.375 to 0.375
- entry_valve_matrix: bfloat16 [2, 8, 256, 256], P(None, 'tp'), may hold values from -0.375 to 0.375
- forgetting_parameters: float32 [2, 2048], P(None, 'tp'), may hold values from 3 to 15
- timestep_forgetting_multiplier: float32 [24576], P(('grp', 'sp')), parts along dimension 0, may hold values from 0.5 to 2
- spike_extra: float32 [24576, 2048], P(('grp', 'sp'), 'tp'), parts along dimension 0, may hold values from -0.7 to 0
- exit_projector_matrix: bfloat16 [2, 2048, 2048], P(None, 'tp', 'sp'), may hold values from -0.125 to 0.125
- prelude_rms_gains: float32 [2, 2048], replicated, may hold values from 0.1 to 1.9
- finishing_rms_gains: float32 [2048], P('tp'), may hold values from 0.1 to 1.9
Outputs:
- result: bfloat16 [24576, 2048], P(('grp', 'sp'), 'tp'), parts along dimension 0
There are 2 independent parts, one for each index of `grp`. A program takes and returns all parts, laid end to end along the dimension named above; an argument that names none is the same for every part. Nothing has to cross between parts.
All inputs are finite; a program needn't handle non-finite values.
Results may differ from a plain program's by a relative error of at most 0.015.
Values may be sent and summed in bfloat16 or wider, within the bound.
A program may use at most 64 MiB of HBM per device.

v0:
```python
import jax
import jax.numpy as jnp
from jax import lax
from jax.sharding import PartitionSpec as P

BLOCK_W = 256
EPSILON = 1e-06
SQUASH_POWER = 8.0


def sent_to_all(x, axis):
    copies = jnp.broadcast_to(x, (lax.axis_size(axis), *x.shape))
    return lax.all_to_all(copies, axis, split_axis=0, concat_axis=0, tiled=True)


def laid_out(tiles, dim):
    lengths = list(tiles.shape[1:])
    lengths[dim] *= tiles.shape[0]
    return jnp.moveaxis(tiles, 0, dim).reshape(lengths)


def gather_directly(x, axis, dim):
    tiles = sent_to_all(x, axis)
    return laid_out(tiles, dim)


def in_one_piece(arrays, axis, dim, along):
    widths = [a.shape[along] for a in arrays]
    both = jnp.concatenate(arrays, axis=along)
    whole = lax.all_gather(both, axis, axis=dim, tiled=True)
    return tuple(jnp.split(whole, [sum(widths[:k]) for k in range(1, len(widths))], axis=along))


def from_behind(value, axis, steps):
    count = lax.axis_size(axis)
    first, last = (max(0, -steps), min(count, count - steps))
    return lax.ppermute(value, axis, [(source, source + steps) for source in range(first, last)])


def gathered_once(x, axis):
    leaves = jax.tree.leaves(x)
    turns = sorted(range(len(leaves)), key=lambda k: -leaves[k].size)
    width = (1, *leaves[turns[0]].shape)[-1]
    lines = [
        jnp.pad(leaves[k].reshape(-1), (0, -leaves[k].size % width)).reshape(-1, width)
        for k in turns
    ]
    both, at, found = (lax.all_gather(jnp.concatenate(lines), axis), 0, {})
    for k, line in zip(turns, lines):
        slab = both[:, at : at + len(line)].reshape(len(both), -1)
        found[k] = slab[:, : leaves[k].size].reshape(-1, *leaves[k].shape)
        at += len(line)
    numbers = iter(range(len(leaves)))
    return jax.tree.map(lambda _: found[next(numbers)], x)


def carried_in(part, axis, combine, identity):
    place = lax.axis_index(axis)
    gathered = gathered_once(part, axis)
    state = jax.tree.map(lambda a, e: jnp.zeros_like(a) + jnp.asarray(e, a.dtype), part, identity)

    def one(lap, state):
        return combine(
            state, jax.tree.map(lambda a: lax.dynamic_index_in_dim(a, lap, 0, False), gathered)
        )

    return lax.fori_loop(0, place, one, state)


def split_up(x, dim, count):
    before, after = (x.shape[:dim], x.shape[dim + 1 :])
    return jnp.moveaxis(x.reshape(*before, count, -1, *after), dim, 0)


def summed_on_arrival(x, axis, dim):
    tiles = split_up(x, dim, lax.axis_size(axis))
    arrived = lax.all_to_all(tiles, axis, split_axis=0, concat_axis=0, tiled=True)
    return arrived.astype(jnp.float32).sum(axis=0)


def of_everyone(x, axis):
    everything = sent_to_all(x, axis)
    return jnp.sum(everything, axis=0)


def combine_pairs(earlier, later):
    return (earlier[0] * later[0], later[0] * earlier[1] + later[1])


def gather_rows(own_cols):
    return gather_directly(own_cols, "tp", 1)


def fetch_layer(multiplier_matrix, memory_path_matrix, exit_projector_matrix, tier_number):
    in_pair = in_one_piece(
        (multiplier_matrix[tier_number], memory_path_matrix[tier_number]), "sp", 0, 1
    )
    out_full = lax.all_gather(exit_projector_matrix[tier_number], "sp", axis=1, tiled=True)
    return (in_pair[0], in_pair[1], out_full)


def on_device(
    starting_stream,
    multiplier_matrix,
    memory_path_matrix,
    filter_coefficients,
    memory_valve_matrix,
    entry_valve_matrix,
    forgetting_parameters,
    timestep_forgetting_multiplier,
    spike_extra,
    exit_projector_matrix,
    prelude_rms_gains,
    finishing_rms_gains,
):
    tok_rows = starting_stream.shape[0]
    channels = memory_path_matrix.shape[2]
    own_cols = starting_stream
    full_rows = gather_rows(starting_stream)
    fetched = fetch_layer(multiplier_matrix, memory_path_matrix, exit_projector_matrix, 0)
    for tier_number in range(memory_path_matrix.shape[0]):
        floats = full_rows.astype(jnp.float32)
        mean_square = jnp.mean(floats * floats, axis=1, keepdims=True)
        normed = (
            floats * lax.rsqrt(mean_square + EPSILON) * prelude_rms_gains[tier_number][None, :]
        ).astype(jnp.bfloat16)
        branch_acc = jnp.dot(normed, fetched[0], preferred_element_type=jnp.float32)
        recur_acc = jnp.dot(normed, fetched[1], preferred_element_type=jnp.float32)
        out_full = fetched[2]
        if tier_number + 1 < memory_path_matrix.shape[0]:
            fetched = fetch_layer(
                multiplier_matrix, memory_path_matrix, exit_projector_matrix, tier_number + 1
            )
        branch = branch_acc.astype(jnp.bfloat16)
        recurrent = recur_acc.astype(jnp.bfloat16)
        taps_now = filter_coefficients[tier_number]
        reach_back = taps_now.shape[0] - 1
        halo_rows = from_behind(recurrent[tok_rows - reach_back :], "sp", 1)
        extended = jnp.concatenate([halo_rows, recurrent], axis=0)
        conv_sum = jnp.zeros((tok_rows, channels), jnp.float32)
        for offset in range(taps_now.shape[0]):
            conv_sum = conv_sum + extended[offset : offset + tok_rows].astype(
                jnp.float32
            ) * taps_now[offset].astype(jnp.float32)
        convolved = conv_sum.astype(jnp.bfloat16)
        blocks = convolved.reshape(tok_rows, channels // BLOCK_W, BLOCK_W)
        reset_gate = jax.nn.sigmoid(
            jnp.einsum(
                "tnc,ncd->tnd",
                blocks,
                memory_valve_matrix[tier_number],
                preferred_element_type=jnp.float32,
            ).reshape(tok_rows, channels)
        )
        inject = jax.nn.sigmoid(
            jnp.einsum(
                "tnc,ncd->tnd",
                blocks,
                entry_valve_matrix[tier_number],
                preferred_element_type=jnp.float32,
            ).reshape(tok_rows, channels)
        )
        logarithmic_persistence = (
            -SQUASH_POWER
            * reset_gate
            * jax.nn.softplus(-forgetting_parameters[tier_number])[None, :]
            * timestep_forgetting_multiplier[:, None]
            + spike_extra
        )
        keep_rate = jnp.exp(logarithmic_persistence)
        driven = (
            inject
            * convolved.astype(jnp.float32)
            * jnp.sqrt(-jnp.expm1(2.0 * logarithmic_persistence))
        )
        keep_cum, state_local = lax.associative_scan(combine_pairs, (keep_rate, driven), axis=0)
        identity = (jnp.ones((channels,), jnp.float32), jnp.zeros((channels,), jnp.float32))
        carried = carried_in((keep_cum[-1], state_local[-1]), "sp", combine_pairs, identity)
        state_seq = state_local + keep_cum * carried[1][None, :]
        mixed_in = (jax.nn.gelu(branch.astype(jnp.float32)) * state_seq).astype(jnp.bfloat16)
        partial_value = jnp.dot(mixed_in, out_full, preferred_element_type=jnp.float32)
        mixed_sum = summed_on_arrival(partial_value.astype(jnp.bfloat16), "tp", 1)
        own_cols = (own_cols.astype(jnp.float32) + mixed_sum).astype(jnp.bfloat16)
        if tier_number + 1 < memory_path_matrix.shape[0]:
            full_rows = gather_rows(own_cols)
    floats = own_cols.astype(jnp.float32)
    full_width = floats.shape[1] * lax.axis_size("tp")
    square_sum = of_everyone(jnp.sum(floats * floats, axis=1), "tp")
    inv_rms = lax.rsqrt(square_sum / full_width + EPSILON)
    return (floats * inv_rms[:, None] * finishing_rms_gains[None, :]).astype(jnp.bfloat16)


def solution(mesh):
    return jax.shard_map(
        on_device,
        mesh=mesh,
        in_specs=(
            P(("grp", "sp"), "tp"),
            P(None, "sp", "tp"),
            P(None, "sp", "tp"),
            P(None, None, "tp"),
            P(None, "tp", None, None),
            P(None, "tp", None, None),
            P(None, "tp"),
            P(("grp", "sp")),
            P(("grp", "sp"), "tp"),
            P(None, "tp", "sp"),
            P(),
            P("tp"),
        ),
        out_specs=P(("grp", "sp"), "tp"),
        check_vma=False,
    )
```

profile of v0, /device:TPU:33, one launch (start us, length us, event | category | flops | bytes accessed | tf_op | source)
XLA Modules:
  0.0 602.2 jit_solution(12787368369105031495)
XLA Ops:
  6.6 0.8 slice_bitcast_fusion
  8.1 1.4 fusion.135
  9.6 1.1 copy.23
  10.7 1.3 broadcast_in_dim.6
  12.0 45.1 %all-to-all-start = ((bf16[8,384,256]{1,2,0:T(8,128)(2,1)}), bf16[8,384,256]{1,2,0:T(8,128)(2,1)S(1)}, u32[]{:S(2)}, u32[]{:S(2)}) async-start(bf16[8,384,256]{1,2,0:T(8,128)(2,1)} %broadcast_in_dim.6), calls=%async_computation | async-start | bytes 3145728 | tf_op jit(solution)/shard_map/all_to_all | solution.py:13
  59.1 18.7 %all-to-all-done = bf16[8,384,256]{1,2,0:T(8,128)(2,1)S(1)} async-done(((bf16[8,384,256]{1,2,0:T(8,128)(2,1)}), bf16[8,384,256]{1,2,0:T(8,128)(2,1)S(1)}, u32[]{:S(2)}, u32[]{:S(2)}) %all-to-all-start) | async-done | bytes 1572896 | tf_op jit(solution)/shard_map/all_to_all | solution.py:13
  78.6 72.2 %all-gather.11.cloned.1.call-done = bf16[2048,512]{1,0:T(8,128)(2,1)} async-done(((bf16[64,512]{1,0:T(8,128)(2,1)}), bf16[2048,512]{1,0:T(8,128)(2,1)}) %all-gather.11.cloned.1.call-update) | async-done | bytes 2097168 | tf_op jit(solution)/shard_map/all_gather | solution.py:30
  150.8 1.8 convolution_convert_fusion.4
  152.7 1.7 collective-permute-start
  174.2 1.5 pad.227
  177.4 40.9 %all-gather.4 = f32[32,2,256]{2,1,0:T(2,128)S(1)} all-gather(f32[1,2,256]{2,1,0:T(2,128)S(1)} %maximum_bitcast_fusion), channel_id=2, replica_groups=mesh['grp'=2,'sp'=32,'tp'=8] {'sp'}, dimensions={0}, use_global_device_ids=true | all-gather | bytes 67584 | tf_op jit(solution)/shard_map/all_gather | solution.py:48
  218.4 59.8 %all-gather.15.cloned.1.call-done = bf16[1,256,2048]{1,2,0:T(8,128)(2,1)} async-done(((bf16[1,256,64]{1,2,0:T(8,128)(2,1)}), bf16[1,256,2048]{1,2,0:T(8,128)(2,1)}) %all-gather.15.cloned.1.call-update) | async-done | bytes 1048592 | tf_op jit(solution)/shard_map/all_gather | solution.py:98
  278.2 3.8 convolution_convert_fusion.1
  282.1 46.2 %all_to_all.26 = bf16[8,384,256]{2,1,0:T(8,128)(2,1)S(1)} all-to-all(bf16[8,384,256]{2,1,0:T(8,128)(2,1)S(1)} %bitcast.108), channel_id=1, replica_groups=mesh['grp'=2,'sp'=32,'tp'=8] {'tp'}, dimensions={0} | all-to-all | bytes 3145728 | tf_op jit(solution)/shard_map/all_to_all | solution.py:77
  329.5 1.3 broadcast_in_dim.7
  330.8 4.5 all-to-all-start.2
  335.9 20.1 %all-to-all-done.2 = bf16[8,384,256]{1,2,0:T(8,128)(2,1)S(1)} async-done(((bf16[8,384,256]{1,2,0:T(8,128)(2,1)}), bf16[8,384,256]{1,2,0:T(8,128)(2,1)S(1)}, u32[]{:S(2)}, u32[]{:S(2)}) %all-to-all-start.2) | async-done | bytes 1572896 | tf_op jit(solution)/shard_map/all_to_all | solution.py:13
  356.9 52.8 %all-gather.13.cloned.1.call-done = bf16[2048,512]{1,0:T(8,128)(2,1)} async-done(((bf16[64,512]{1,0:T(8,128)(2,1)}), bf16[2048,512]{1,0:T(8,128)(2,1)}) %all-gather.13.cloned.1.call-update) | async-done | bytes 2097168 | tf_op jit(solution)/shard_map/all_gather | solution.py:30
  409.7 1.8 convolution_convert_fusion.2
  411.6 1.5 collective-permute-start.1
  414.2 1.3 fusion.22
  415.9 0.8 slice.719
  416.7 1.0 multiply_add_fusion.2
  440.9 0.8 fusion.105
  443.3 1.6 pad.259
  446.4 1.7 pad.242
  448.8 41.6 %all-gather.5 = f32[32,2,256]{2,1,0:T(2,128)S(1)} all-gather(f32[1,2,256]{2,1,0:T(2,128)S(1)} %maximum_bitcast_fusion.1), channel_id=4, replica_groups=mesh['grp'=2,'sp'=32,'tp'=8] {'sp'}, dimensions={0}, use_global_device_ids=true | all-gather | bytes 67584 | tf_op jit(solution)/shard_map/all_gather | solution.py:48
  490.5 45.1 %all-gather.17.cloned.1.call-done = bf16[1,256,2048]{1,2,0:T(8,128)(2,1)} async-done(((bf16[1,256,64]{1,2,0:T(8,128)(2,1)}), bf16[1,256,2048]{1,2,0:T(8,128)(2,1)}) %all-gather.17.cloned.1.call-update) | async-done | bytes 1048592 | tf_op jit(solution)/shard_map/all_gather | solution.py:98
  535.7 3.9 convolution_convert_fusion
  539.7 46.7 %all_to_all.27 = bf16[8,384,256]{2,1,0:T(8,128)(2,1)S(1)} all-to-all(bf16[8,384,256]{2,1,0:T(8,128)(2,1)S(1)} %bitcast.109), channel_id=1, replica_groups=mesh['grp'=2,'sp'=32,'tp'=8] {'tp'}, dimensions={0} | all-to-all | bytes 3145728 | tf_op jit(solution)/shard_map/all_to_all | solution.py:77
  586.7 8.1 %all_to_all.28 = f32[8,1,384]{2,1,0:T(1,128)S(1)} all-to-all(f32[8,1,384]{2,1,0:T(1,128)S(1)} %broadcast_in_dim.8), channel_id=1, replica_groups=mesh['grp'=2,'sp'=32,'tp'=8] {'tp'}, dimensions={0} | all-to-all | bytes 24576 | tf_op jit(solution)/shard_map/all_to_all | solution.py:13
  594.9 0.8 fusion.36
  (388 shorter events, 55.8 us)
Async XLA Ops:
  6.5 144.2 %all-gather.11.cloned.1.call-start = ((), (), s32[]{:S(2)}) async-start(), calls=%async_computation.5 | async-start | bytes 2162688 | tf_op jit(solution)/shard_map/all_gather | solution.py:30
  8.1 270.1 %all-gather.15.cloned.1.call-start = ((), (), s32[]{:S(2)}) async-start(), calls=%async_computation.7 | async-start | bytes 1081344 | tf_op jit(solution)/shard_map/all_gather | solution.py:98
  12.0 45.8 %copy-start.28 = (f32[2,256]{1,0:T(2,128)S(1)}, f32[2,256]{1,0:T(2,128)}, u32[]{:S(2)}) copy-start(f32[2,256]{1,0:T(2,128)} %param.22) | copy-start | bytes 6148
  12.0 46.4 %copy-start.11 = (bf16[2,4,256]{2,1,0:T(4,128)(2,1)S(1)}, bf16[2,4,256]{2,1,0:T(4,128)(2,1)}, u32[]{:S(2)}) copy-start(bf16[2,4,256]{2,1,0:T(4,128)(2,1)} %param.19) | copy-start | bytes 12292
  12.0 47.0 %copy-start.10 = (f32[2,2048]{1,0:T(2,128)S(1)}, f32[2,2048]{1,0:T(2,128)}, u32[]{:S(2)}) copy-start(f32[2,2048]{1,0:T(2,128)} %param.26) | copy-start | bytes 49156
  12.0 65.7 %all-to-all-start = ((bf16[8,384,256]{1,2,0:T(8,128)(2,1)}), bf16[8,384,256]{1,2,0:T(8,128)(2,1)S(1)}, u32[]{:S(2)}, u32[]{:S(2)}) async-start(bf16[8,384,256]{1,2,0:T(8,128)(2,1)} %broadcast_in_dim.6), calls=%async_computation | async-start | bytes 3145728 | tf_op jit(solution)/shard_map/all_to_all | solution.py:13
  57.1 352.6 %all-gather.13.cloned.1.call-start = ((), (), s32[]{:S(2)}) async-start(), calls=%async_computation.6 | async-start | bytes 2162688 | tf_op jit(solution)/shard_map/all_gather | solution.py:30
  78.6 76.7 %copy-start.31 = (f32[384,256]{1,0:T(8,128)S(1)}, f32[384,256]{1,0:T(8,128)}, u32[]{:S(2)}) copy-start(f32[384,256]{1,0:T(8,128)} %param.24) | copy-start | bytes 1179652
  78.6 76.7 %copy-start.33 = (bf16[2,1,256,256]{3,2,1,0:T(8,128)(2,1)S(1)}, bf16[2,1,256,256]{3,2,1,0:T(8,128)(2,1)}, u32[]{:S(2)}) copy-start(bf16[2,1,256,256]{3,2,1,0:T(8,128)(2,1)} %param.20) | copy-start | bytes 786436
  78.6 76.7 %copy-start.36 = (f32[384]{0:T(512)S(1)}, f32[384]{0:T(512)}, u32[]{:S(2)}) copy-start(f32[384]{0:T(512)} %param.23) | copy-start | bytes 4612
  152.7 2.5 collective-permute-start
  156.1 11.2 %copy-start = (f32[384,256]{1,0:T(8,128)}, f32[384,256]{1,0:T(8,128)S(1)}, u32[]{:S(2)}) copy-start(f32[384,256]{1,0:T(8,128)S(1)} %fusion.25) | copy-start | bytes 1179652
  176.5 101.7 %copy-start.5 = (f32[384,256]{1,0:T(8,128)}, f32[384,256]{1,0:T(8,128)S(1)}, u32[]{:S(2)}) copy-start(f32[384,256]{1,0:T(8,128)S(1)} %pad.226) | copy-start | bytes 1179652
  177.2 101.0 %copy-start.6 = (f32[384,256]{1,0:T(8,128)}, f32[384,256]{1,0:T(8,128)S(1)}, u32[]{:S(2)}) copy-start(f32[384,256]{1,0:T(8,128)S(1)} %pad.211) | copy-start | bytes 1179652
  330.8 25.2 %all-to-all-start.2 = ((bf16[8,384,256]{1,2,0:T(8,128)(2,1)}), bf16[8,384,256]{1,2,0:T(8,128)(2,1)S(1)}, u32[]{:S(2)}, u32[]{:S(2)}) async-start(bf16[8,384,256]{1,2,0:T(8,128)(2,1)} %broadcast_in_dim.7), calls=%async_computation.2 | async-start | bytes 3145728 | tf_op jit(solution)/shard_map/all_to_all | solution.py:13
  335.3 200.3 %all-gather.17.cloned.1.call-start = ((), (), s32[]{:S(2)}) async-start(), calls=%async_computation.8 | async-start | bytes 1081344 | tf_op jit(solution)/shard_map/all_gather | solution.py:98
  356.8 56.7 %copy-start.12 = (f32[1,1,256]{2,1,0:T(1,128)S(1)}, f32[1,1,256]{2,1,0:T(1,128)}, u32[]{:S(2)}) copy-start(f32[1,1,256]{2,1,0:T(1,128)} %get-tuple-element.193) | copy-start | bytes 3076
  356.9 56.7 %copy-start.13 = (f32[1,1,256]{2,1,0:T(1,128)S(1)}, f32[1,1,256]{2,1,0:T(1,128)}, u32[]{:S(2)}) copy-start(f32[1,1,256]{2,1,0:T(1,128)} %get-tuple-element.194) | copy-start | bytes 3076
  356.9 56.7 %copy-start.14 = (f32[1,1,256]{2,1,0:T(1,128)S(1)}, f32[1,1,256]{2,1,0:T(1,128)}, u32[]{:S(2)}) copy-start(f32[1,1,256]{2,1,0:T(1,128)} %get-tuple-element.199) | copy-start | bytes 3076
  356.9 56.7 %copy-start.15 = (f32[1,1,256]{2,1,0:T(1,128)S(1)}, f32[1,1,256]{2,1,0:T(1,128)}, u32[]{:S(2)}) copy-start(f32[1,1,256]{2,1,0:T(1,128)} %get-tuple-element.200) | copy-start | bytes 3076
  356.9 56.9 %copy-start.30 = (f32[1,256]{1,0:T(1,128)S(1)}, f32[1,256]{1,0:T(1,128)}, u32[]{:S(2)}) copy-start(f32[1,256]{1,0:T(1,128)} %get-tuple-element.209) | copy-start | bytes 3076
  356.9 56.9 %copy-start.32 = (f32[384,256]{1,0:T(8,128)S(1)}, f32[384,256]{1,0:T(8,128)}, u32[]{:S(2)}) copy-start(f32[384,256]{1,0:T(8,128)} %param.24) | copy-start | bytes 1179652
  356.9 56.9 %copy-start.34 = (bf16[2,1,256,256]{3,2,1,0:T(8,128)(2,1)S(1)}, bf16[2,1,256,256]{3,2,1,0:T(8,128)(2,1)}, u32[]{:S(2)}) copy-start(bf16[2,1,256,256]{3,2,1,0:T(8,128)(2,1)} %param.20) | copy-start | bytes 786436
  356.9 56.9 %copy-start.37 = (f32[384]{0:T(512)S(1)}, f32[384]{0:T(512)}, u32[]{:S(2)}) copy-start(f32[384]{0:T(512)} %param.23) | copy-start | bytes 4612
  411.6 2.0 collective-permute-start.1
  415.5 18.7 %copy-start.1 = (f32[384,256]{1,0:T(8,128)}, f32[384,256]{1,0:T(8,128)S(1)}, u32[]{:S(2)}) copy-start(f32[384,256]{1,0:T(8,128)S(1)} %fusion.22) | copy-start | bytes 1179652
  432.5 8.2 %copy-start.25 = (f32[1,256]{1,0:T(1,128)S(1)}, f32[1,256]{1,0:T(1,128)}, u32[]{:S(2)}) copy-start(f32[1,256]{1,0:T(1,128)} %slice.887) | copy-start | bytes 3076
  432.5 8.3 %copy-start.23 = (f32[1,256]{1,0:T(1,128)S(1)}, f32[1,256]{1,0:T(1,128)}, u32[]{:S(2)}) copy-start(f32[1,256]{1,0:T(1,128)} %slice.861) | copy-start | bytes 3076
  432.5 8.4 %copy-start.7 = (f32[47,256]{1,0:T(8,128)S(1)}, f32[47,256]{1,0:T(8,128)}, u32[]{:S(2)}) copy-start(f32[47,256]{1,0:T(8,128)} %slice.769) | copy-start | bytes 144388
  445.6 90.0 %copy-start.3 = (f32[384,256]{1,0:T(8,128)}, f32[384,256]{1,0:T(8,128)S(1)}, u32[]{:S(2)}) copy-start(f32[384,256]{1,0:T(8,128)S(1)} %pad.258) | copy-start | bytes 1179652
  446.4 89.3 %copy-start.4 = (f32[384,256]{1,0:T(8,128)}, f32[384,256]{1,0:T(8,128)S(1)}, u32[]{:S(2)}) copy-start(f32[384,256]{1,0:T(8,128)S(1)} %pad.243) | copy-start | bytes 1179652
  586.3 8.5 %copy-start.29 = (f32[256]{0:T(256)S(1)}, f32[256]{0:T(256)}, u32[]{:S(2)}) copy-start(f32[256]{0:T(256)} %param.27) | copy-start | bytes 3076
  (16 other events, 60.6 us)
Sparse Core Ops, SparseCore 0:
  9.4 141.3 all-gather.10
  152.9 125.2 all-gather.14
  280.3 129.3 all-gather.12
  411.6 123.9 all-gather.16
where the time goes:
time: 604 us; the launch traced here: 602 us
  waiting for transfers between devices  271 us (45%)
  blocking collectives  183 us (30%)
  starting transfers between devices  52.9 us (9%)
  local copies, waits for them, and re-layouts  42.2 us (7%)
  other arithmetic  24.4 us (4%)
  between operations  14.8 us (2%)
  matrix products  13.7 us (2%)
    all_gather x2, waiting for transfers between devices, in_one_piece(): whole = lax.all_gather(both, axis, axis=dim, tiled=True)  125 us
    all_gather x2, waiting for transfers between devices, fetch_layer(): lax.all_gather(exit_projector_matrix[tier_number], 'sp', axis=1, tiled=True)  105 us
    all_to_all x2, blocking collectives, summed_on_arrival(): lax.all_to_all(tiles, axis, split_axis=0, concat_axis=0, tiled=True)  92.9 us
    all_gather x2, blocking collectives, gathered_once(): both, at, found = (lax.all_gather(jnp.concatenate(lines), axis), 0, {})  82.5 us
    all_to_all x2, starting transfers between devices, sent_to_all(): return lax.all_to_all(copies, axis, split_axis=0, concat_axis=0, tiled=True)  49.6 us
    all_to_all x2, waiting for transfers between devices, sent_to_all(): return lax.all_to_all(copies, axis, split_axis=0, concat_axis=0, tiled=True)  38.8 us
    slice x114, local copies, waits for them, and re-layouts, on_device(): lax.associative_scan(combine_pairs, (keep_rate, driven), axis=0)  28.4 us
  transfers between devices with their start and end apart: 8, of which 8 were waited for; matrix products, arithmetic and copies ran while one was open for 12% of the time, Pallas kernels for 0%

commit v1 on v0

--- a/solution.py
+++ b/solution.py
@@ -95,7 +95,11 @@
     in_pair = in_one_piece(
         (multiplier_matrix[tier_number], memory_path_matrix[tier_number]), "sp", 0, 1
     )
-    out_full = lax.all_gather(exit_projector_matrix[tier_number], "sp", axis=1, tiled=True)
+    array = exit_projector_matrix[tier_number]
+    n_dev = lax.axis_size("sp")
+    pieces = jnp.stack([array for _ in range(n_dev)])
+    pieces = lax.all_to_all(pieces, "sp", split_axis=0, concat_axis=0)
+    out_full = jnp.concatenate(pieces, axis=1)
     return (in_pair[0], in_pair[1], out_full)
 
 

time: 604 us -> 647 us (1.071)
  starting transfers between devices: 52.9 us -> 108 us
  blocking collectives: 183 us -> 167 us
    all_gather x2, waiting for transfers between devices: 125 us -> 233 us  [in_one_piece(): whole = lax.all_gather(both, axis, axis=dim, tiled=True)]
    all_gather x2 -> x0, waiting for transfers between devices: 105 us -> none  [fetch_layer(): lax.all_gather(exit_projector_matrix[tier_number], 'sp', axis=1, tiled=True)]
    all_to_all x0 -> x3, starting transfers between devices: none -> 56.2 us  [the longest x1 33.9 us: summed_on_arrival(): lax.all_to_all(tiles, axis, split_axis=0, concat_axis=0, tiled=True)]
    all_to_all x2 -> x1, blocking collectives: 92.9 us -> 53.9 us  [summed_on_arrival(): lax.all_to_all(tiles, axis, split_axis=0, concat_axis=0, tiled=True)]
    all_to_all x1 -> x2, blocking collectives: 8.1 us -> 32.1 us  [sent_to_all(): return lax.all_to_all(copies, axis, split_axis=0, concat_axis=0, tiled=True)]
    all_to_all x2 -> x1, waiting for transfers between devices: 38.8 us -> 18.9 us  [sent_to_all(): return lax.all_to_all(copies, axis, split_axis=0, concat_axis=0, tiled=True)]
    all_to_all x0 -> x3, waiting for transfers between devices: none -> 19.8 us  [the longest x1 19.8 us: summed_on_arrival(): lax.all_to_all(tiles, axis, split_axis=0, concat_axis=0, tiled=True)]
    all_to_all x2 -> x1, starting transfers between devices: 49.6 us -> 45.1 us  [sent_to_all(): return lax.all_to_all(copies, axis, split_axis=0, concat_axis=0, tiled=True)]
  transfers between devices with their start and end apart: 8 -> 8, of which waited for: 8 -> 6; matrix products, arithmetic and copies ran while one was open for 12% -> 11% of each run, Pallas kernels for 0% -> 0%
where the time goes in v1:
time: 647 us; the launch traced here: 645 us
  waiting for transfers between devices  273 us (42%)
  blocking collectives  167 us (26%)
  starting transfers between devices  108 us (17%)
  local copies, waits for them, and re-layouts  43.6 us (7%)
  other arithmetic  24.3 us (4%)
  between operations  15.2 us (2%)
  matrix products  13.8 us (2%)
    all_gather x2, waiting for transfers between devices, in_one_piece(): whole = lax.all_gather(both, axis, axis=dim, tiled=True)  233 us
    all_gather x2, blocking collectives, gathered_once(): both, at, found = (lax.all_gather(jnp.concatenate(lines), axis), 0, {})  80.6 us
    all_to_all x1, blocking collectives, summed_on_arrival(): lax.all_to_all(tiles, axis, split_axis=0, concat_axis=0, tiled=True)  53.9 us
    all_to_all x1, starting transfers between devices, sent_to_all(): return lax.all_to_all(copies, axis, split_axis=0, concat_axis=0, tiled=True)  45.1 us
    all_to_all x1, starting transfers between devices, summed_on_arrival(): lax.all_to_all(tiles, axis, split_axis=0, concat_axis=0, tiled=True)  33.9 us
    all_to_all x2, blocking collectives, sent_to_all(): return lax.all_to_all(copies, axis, split_axis=0, concat_axis=0, tiled=True)  32.1 us
    slice x114, local copies, waits for them, and re-layouts, on_device(): lax.associative_scan(combine_pairs, (keep_rate, driven), axis=0)  28.3 us
    all_to_all x2, starting transfers between devices, fetch_layer(): pieces = lax.all_to_all(pieces, 'sp', split_axis=0, concat_axis=0)  22.3 us
  transfers between devices with their start and end apart: 8, of which 6 were waited for; matrix products, arithmetic and copies ran while one was open for 11% of the time, Pallas kernels for 0%

profile of v1, /device:TPU:33, one launch (start us, length us, event | category | flops | bytes accessed | tf_op | source)
XLA Modules:
  0.0 644.9 jit_solution(461318313953870708)
XLA Ops:
  6.6 1.4 slice_bitcast_fusion.1
  8.7 1.1 copy.25
  9.8 1.3 broadcast_in_dim.6
  11.1 45.1 %all-to-all-start = ((bf16[8,384,256]{1,2,0:T(8,128)(2,1)}), bf16[8,384,256]{1,2,0:T(8,128)(2,1)S(1)}, u32[]{:S(2)}, u32[]{:S(2)}) async-start(bf16[8,384,256]{1,2,0:T(8,128)(2,1)} %broadcast_in_dim.6), calls=%async_computation | async-start | bytes 3145728 | tf_op jit(solution)/shard_map/all_to_all | solution.py:13
  57.9 18.9 %all-to-all-done = bf16[8,384,256]{1,2,0:T(8,128)(2,1)S(1)} async-done(((bf16[8,384,256]{1,2,0:T(8,128)(2,1)}), bf16[8,384,256]{1,2,0:T(8,128)(2,1)S(1)}, u32[]{:S(2)}, u32[]{:S(2)}) %all-to-all-start) | async-done | bytes 1572896 | tf_op jit(solution)/shard_map/all_to_all | solution.py:13
  76.8 1.1 stack.6
  77.9 6.5 %all-to-all-start.1 = ((bf16[32,256,64]{1,2,0:T(8,128)(2,1)}), bf16[32,256,64]{1,2,0:T(8,128)(2,1)}, u32[]{:S(2)}, u32[]{:S(2)}) async-start(bf16[32,256,64]{1,2,0:T(8,128)(2,1)} %stack.6), calls=%async_computation.1 | async-start | bytes 2097152 | tf_op jit(solution)/shard_map/all_to_all | solution.py:101
  85.3 124.7 %all-gather.7.cloned.1.call-done = bf16[2048,512]{1,0:T(8,128)(2,1)} async-done(((bf16[64,512]{1,0:T(8,128)(2,1)}), bf16[2048,512]{1,0:T(8,128)(2,1)}) %all-gather.7.cloned.1.call-update) | async-done | bytes 2097168 | tf_op jit(solution)/shard_map/all_gather | solution.py:30
  210.0 1.8 convolution_convert_fusion.4
  211.9 2.6 collective-permute-start
  234.4 1.6 pad.227
  237.6 40.9 %all-gather.2 = f32[32,2,256]{2,1,0:T(2,128)S(1)} all-gather(f32[1,2,256]{2,1,0:T(2,128)S(1)} %maximum_bitcast_fusion), channel_id=2, replica_groups=mesh['grp'=2,'sp'=32,'tp'=8] {'sp'}, dimensions={0}, use_global_device_ids=true | all-gather | bytes 67584 | tf_op jit(solution)/shard_map/all_gather | solution.py:48
  278.6 3.8 convolution_convert_fusion.1
  282.4 1.3 copy.44
  283.7 33.9 %all-to-all-start.2 = ((bf16[8,384,256]{2,1,0:T(8,128)(2,1)}), bf16[8,384,256]{2,1,0:T(8,128)(2,1)S(1)}, u32[]{:S(2)}, u32[]{:S(2)}) async-start(bf16[8,384,256]{2,1,0:T(8,128)(2,1)} %bitcast.101), calls=%async_computation.2 | async-start | bytes 3145728 | tf_op jit(solution)/shard_map/all_to_all | solution.py:77
  318.3 19.8 %all-to-all-done.2 = bf16[8,384,256]{2,1,0:T(8,128)(2,1)S(1)} async-done(((bf16[8,384,256]{2,1,0:T(8,128)(2,1)}), bf16[8,384,256]{2,1,0:T(8,128)(2,1)S(1)}, u32[]{:S(2)}, u32[]{:S(2)}) %all-to-all-start.2) | async-done | bytes 1572896 | tf_op jit(solution)/shard_map/all_to_all | solution.py:77
  338.7 24.0 %all_to_all.36 = bf16[8,384,256]{1,2,0:T(8,128)(2,1)S(1)} all-to-all(bf16[8,384,256]{1,2,0:T(8,128)(2,1)S(1)} %broadcast_in_dim.7), channel_id=1, replica_groups=mesh['grp'=2,'sp'=32,'tp'=8] {'tp'}, dimensions={0} | all-to-all | bytes 3145728 | tf_op jit(solution)/shard_map/all_to_all | solution.py:13
  362.8 1.1 stack.7
  363.9 15.8 %all-to-all-start.4 = ((bf16[32,256,64]{1,2,0:T(8,128)(2,1)}), bf16[32,256,64]{1,2,0:T(8,128)(2,1)}, u32[]{:S(2)}, u32[]{:S(2)}) async-start(bf16[32,256,64]{1,2,0:T(8,128)(2,1)} %stack.7), calls=%async_computation.4 | async-start | bytes 2097152 | tf_op jit(solution)/shard_map/all_to_all | solution.py:101
  380.6 108.4 %all-gather.9.cloned.1.call-done = bf16[2048,512]{1,0:T(8,128)(2,1)} async-done(((bf16[64,512]{1,0:T(8,128)(2,1)}), bf16[2048,512]{1,0:T(8,128)(2,1)}) %all-gather.9.cloned.1.call-update) | async-done | bytes 2097168 | tf_op jit(solution)/shard_map/all_gather | solution.py:30
  489.1 1.8 convolution_convert_fusion.2
  490.9 4.0 collective-permute-start.1
  496.2 1.3 fusion.22
  498.7 1.0 multiply_add_fusion.2
  523.0 0.8 fusion.103
  525.3 1.6 pad.259
  527.8 1.7 pad.242
  530.9 39.7 %all-gather.3 = f32[32,2,256]{2,1,0:T(2,128)S(1)} all-gather(f32[1,2,256]{2,1,0:T(2,128)S(1)} %maximum_bitcast_fusion.1), channel_id=3, replica_groups=mesh['grp'=2,'sp'=32,'tp'=8] {'sp'}, dimensions={0}, use_global_device_ids=true | all-gather | bytes 67584 | tf_op jit(solution)/shard_map/all_gather | solution.py:48
  570.8 3.9 convolution_convert_fusion
  574.8 53.9 %all_to_all.37 = bf16[8,384,256]{2,1,0:T(8,128)(2,1)S(1)} all-to-all(bf16[8,384,256]{2,1,0:T(8,128)(2,1)S(1)} %bitcast.114), channel_id=1, replica_groups=mesh['grp'=2,'sp'=32,'tp'=8] {'tp'}, dimensions={0} | all-to-all | bytes 3145728 | tf_op jit(solution)/shard_map/all_to_all | solution.py:77
  629.1 8.1 %all_to_all.38 = f32[8,1,384]{2,1,0:T(1,128)S(1)} all-to-all(f32[8,1,384]{2,1,0:T(1,128)S(1)} %broadcast_in_dim.8), channel_id=1, replica_groups=mesh['grp'=2,'sp'=32,'tp'=8] {'tp'}, dimensions={0} | all-to-all | bytes 24576 | tf_op jit(solution)/shard_map/all_to_all | solution.py:13
  637.2 0.8 fusion.34
  (396 shorter events, 56.0 us)
Async XLA Ops:
  6.5 203.5 %all-gather.7.cloned.1.call-start = ((), (), s32[]{:S(2)}) async-start(), calls=%async_computation.7 | async-start | bytes 2162688 | tf_op jit(solution)/shard_map/all_gather | solution.py:30
  11.1 45.1 %copy-start.32 = (f32[2,256]{1,0:T(2,128)S(1)}, f32[2,256]{1,0:T(2,128)}, u32[]{:S(2)}) copy-start(f32[2,256]{1,0:T(2,128)} %param.22) | copy-start | bytes 6148
  11.1 45.6 %copy-start.15 = (bf16[2,4,256]{2,1,0:T(4,128)(2,1)S(1)}, bf16[2,4,256]{2,1,0:T(4,128)(2,1)}, u32[]{:S(2)}) copy-start(bf16[2,4,256]{2,1,0:T(4,128)(2,1)} %param.19) | copy-start | bytes 12292
  11.1 46.2 %copy-start.13 = (bf16[2,256,64]{1,2,0:T(8,128)(2,1)S(1)}, bf16[2,256,64]{1,2,0:T(8,128)(2,1)}, u32[]{:S(2)}) copy-start(bf16[2,256,64]{1,2,0:T(8,128)(2,1)} %param.25) | copy-start | bytes 196612
  11.1 46.8 %copy-start.14 = (f32[2,2048]{1,0:T(2,128)S(1)}, f32[2,2048]{1,0:T(2,128)}, u32[]{:S(2)}) copy-start(f32[2,2048]{1,0:T(2,128)} %param.26) | copy-start | bytes 49156
  11.1 65.7 %all-to-all-start = ((bf16[8,384,256]{1,2,0:T(8,128)(2,1)}), bf16[8,384,256]{1,2,0:T(8,128)(2,1)S(1)}, u32[]{:S(2)}, u32[]{:S(2)}) async-start(bf16[8,384,256]{1,2,0:T(8,128)(2,1)} %broadcast_in_dim.6), calls=%async_computation | async-start | bytes 3145728 | tf_op jit(solution)/shard_map/all_to_all | solution.py:13
  77.9 200.6 %all-to-all-start.1 = ((bf16[32,256,64]{1,2,0:T(8,128)(2,1)}), bf16[32,256,64]{1,2,0:T(8,128)(2,1)}, u32[]{:S(2)}, u32[]{:S(2)}) async-start(bf16[32,256,64]{1,2,0:T(8,128)(2,1)} %stack.6), calls=%async_computation.1 | async-start | bytes 2097152 | tf_op jit(solution)/shard_map/all_to_all | solution.py:101
  85.3 130.2 %copy-start.35 = (f32[384,256]{1,0:T(8,128)S(1)}, f32[384,256]{1,0:T(8,128)}, u32[]{:S(2)}) copy-start(f32[384,256]{1,0:T(8,128)} %param.24) | copy-start | bytes 1179652
  85.3 130.2 %copy-start.37 = (bf16[2,1,256,256]{3,2,1,0:T(8,128)(2,1)S(1)}, bf16[2,1,256,256]{3,2,1,0:T(8,128)(2,1)}, u32[]{:S(2)}) copy-start(bf16[2,1,256,256]{3,2,1,0:T(8,128)(2,1)} %param.20) | copy-start | bytes 786436
  85.3 130.2 %copy-start.40 = (f32[384]{0:T(512)S(1)}, f32[384]{0:T(512)}, u32[]{:S(2)}) copy-start(f32[384]{0:T(512)} %param.23) | copy-start | bytes 4612
  211.9 3.3 collective-permute-start
  236.7 41.9 %copy-start.5 = (f32[384,256]{1,0:T(8,128)}, f32[384,256]{1,0:T(8,128)S(1)}, u32[]{:S(2)}) copy-start(f32[384,256]{1,0:T(8,128)S(1)} %pad.226) | copy-start | bytes 1179652
  236.7 41.9 %copy-start.6 = (f32[384,256]{1,0:T(8,128)}, f32[384,256]{1,0:T(8,128)S(1)}, u32[]{:S(2)}) copy-start(f32[384,256]{1,0:T(8,128)S(1)} %pad.211) | copy-start | bytes 1179652
  283.7 33.9 %copy-start.9 = (bf16[64,256]{1,0:T(8,128)(2,1)S(1)}, bf16[64,256]{1,0:T(8,128)(2,1)}, u32[]{:S(2)}) copy-start(bf16[64,256]{1,0:T(8,128)(2,1)} %get-tuple-element.147) | copy-start | bytes 98308
  283.7 33.9 %copy-start.10 = (bf16[64,256]{1,0:T(8,128)(2,1)S(1)}, bf16[64,256]{1,0:T(8,128)(2,1)}, u32[]{:S(2)}) copy-start(bf16[64,256]{1,0:T(8,128)(2,1)} %get-tuple-element.218) | copy-start | bytes 98308
  283.7 54.4 %all-to-all-start.2 = ((bf16[8,384,256]{2,1,0:T(8,128)(2,1)}), bf16[8,384,256]{2,1,0:T(8,128)(2,1)S(1)}, u32[]{:S(2)}, u32[]{:S(2)}) async-start(bf16[8,384,256]{2,1,0:T(8,128)(2,1)} %bitcast.101), calls=%async_computation.2 | async-start | bytes 3145728 | tf_op jit(solution)/shard_map/all_to_all | solution.py:77
  317.5 20.8 %copy-start.2 = (bf16[384,256]{1,0:T(8,128)(2,1)S(1)}, bf16[384,256]{1,0:T(8,128)(2,1)}, u32[]{:S(2)}) copy-start(bf16[384,256]{1,0:T(8,128)(2,1)} %param.16) | copy-start | bytes 589828
  317.5 171.5 %all-gather.9.cloned.1.call-start = ((), (), s32[]{:S(2)}) async-start(), calls=%async_computation.8 | async-start | bytes 2162688 | tf_op jit(solution)/shard_map/all_gather | solution.py:30
  338.7 24.1 %copy-start.8 = (bf16[256,64]{0,1:T(8,128)(2,1)S(1)}, bf16[256,64]{0,1:T(8,128)(2,1)}, u32[]{:S(2)}) copy-start(bf16[256,64]{0,1:T(8,128)(2,1)} %get-tuple-element.152) | copy-start | bytes 98308
  363.9 206.9 %all-to-all-start.4 = ((bf16[32,256,64]{1,2,0:T(8,128)(2,1)}), bf16[32,256,64]{1,2,0:T(8,128)(2,1)}, u32[]{:S(2)}, u32[]{:S(2)}) async-start(bf16[32,256,64]{1,2,0:T(8,128)(2,1)} %stack.7), calls=%async_computation.4 | async-start | bytes 2097152 | tf_op jit(solution)/shard_map/all_to_all | solution.py:101
  380.5 115.1 %copy-start.16 = (f32[1,1,256]{2,1,0:T(1,128)S(1)}, f32[1,1,256]{2,1,0:T(1,128)}, u32[]{:S(2)}) copy-start(f32[1,1,256]{2,1,0:T(1,128)} %get-tuple-element.193) | copy-start | bytes 3076
  380.6 115.1 %copy-start.17 = (f32[1,1,256]{2,1,0:T(1,128)S(1)}, f32[1,1,256]{2,1,0:T(1,128)}, u32[]{:S(2)}) copy-start(f32[1,1,256]{2,1,0:T(1,128)} %get-tuple-element.194) | copy-start | bytes 3076
  380.6 115.1 %copy-start.18 = (f32[1,1,256]{2,1,0:T(1,128)S(1)}, f32[1,1,256]{2,1,0:T(1,128)}, u32[]{:S(2)}) copy-start(f32[1,1,256]{2,1,0:T(1,128)} %get-tuple-element.199) | copy-start | bytes 3076
  380.6 115.1 %copy-start.19 = (f32[1,1,256]{2,1,0:T(1,128)S(1)}, f32[1,1,256]{2,1,0:T(1,128)}, u32[]{:S(2)}) copy-start(f32[1,1,256]{2,1,0:T(1,128)} %get-tuple-element.200) | copy-start | bytes 3076
  380.6 115.3 %copy-start.34 = (f32[1,256]{1,0:T(1,128)S(1)}, f32[1,256]{1,0:T(1,128)}, u32[]{:S(2)}) copy-start(f32[1,256]{1,0:T(1,128)} %get-tuple-element.209) | copy-start | bytes 3076
  380.6 115.3 %copy-start.36 = (f32[384,256]{1,0:T(8,128)S(1)}, f32[384,256]{1,0:T(8,128)}, u32[]{:S(2)}) copy-start(f32[384,256]{1,0:T(8,128)} %param.24) | copy-start | bytes 1179652
  380.6 115.3 %copy-start.38 = (bf16[2,1,256,256]{3,2,1,0:T(8,128)(2,1)S(1)}, bf16[2,1,256,256]{3,2,1,0:T(8,128)(2,1)}, u32[]{:S(2)}) copy-start(bf16[2,1,256,256]{3,2,1,0:T(8,128)(2,1)} %param.20) | copy-start | bytes 786436
  380.6 115.3 %copy-start.41 = (f32[384]{0:T(512)S(1)}, f32[384]{0:T(512)}, u32[]{:S(2)}) copy-start(f32[384]{0:T(512)} %param.23) | copy-start | bytes 4612
  490.9 4.7 collective-permute-start.1
  497.5 18.7 %copy-start.1 = (f32[384,256]{1,0:T(8,128)}, f32[384,256]{1,0:T(8,128)S(1)}, u32[]{:S(2)}) copy-start(f32[384,256]{1,0:T(8,128)S(1)} %fusion.22) | copy-start | bytes 1179652
  527.7 43.1 %copy-start.3 = (f32[384,256]{1,0:T(8,128)}, f32[384,256]{1,0:T(8,128)S(1)}, u32[]{:S(2)}) copy-start(f32[384,256]{1,0:T(8,128)S(1)} %pad.258) | copy-start | bytes 1179652
  527.7 43.1 %copy-start.4 = (f32[384,256]{1,0:T(8,128)}, f32[384,256]{1,0:T(8,128)S(1)}, u32[]{:S(2)}) copy-start(f32[384,256]{1,0:T(8,128)S(1)} %pad.243) | copy-start | bytes 1179652
  (20 other events, 104.2 us)
Sparse Core Ops, SparseCore 0:
  9.4 200.5 all-gather.6
  320.4 168.5 all-gather.8
